TPU v7x, 256 devices: a 2x2x32 block of a 4x16x32 slice. The times are simulated.
256 devices in a mesh: grp: 4 (over y, x), ep: 32 (over z), tp: 2 (over core).
Axes of the slice: x: 2, y: 2, z: 32, core: 2. Of those that a mesh axis runs over, the one named last changes fastest.
The devices are a block of a 4x16x32 slice.
Arguments:
- tokens: bfloat16 [32768, 2048], P(('grp', 'ep', 'tp')), parts along dimension 0, may hold values from -6 to 6
- expert_ids: int32 [32768, 4], P(('grp', 'ep', 'tp')), parts along dimension 0, may hold values from 0 to 63, all different within a row; in each aligned block of 128 rows (0 to 127, 128 to 255, ...) at most 16 rows name the same one
- route_weights: float32 [32768, 4], P(('grp', 'ep', 'tp')), parts along dimension 0, may hold values from 0.05 to 1
- norm_gain: float32 [2048], replicated, may hold values from 0.1 to 1.9
- w_gate: bfloat16 [64, 2048, 896], P(('ep', 'tp')), may hold values from -0.5 to 0.5
- w_up: bfloat16 [64, 2048, 896], P(('ep', 'tp')), may hold values from -0.5 to 0.5
- w_down: bfloat16 [64, 896, 2048], P(('ep', 'tp')), may hold values from -0.0234375 to 0.0234375
Outputs:
- mixed: bfloat16 [32768, 2048], P(('grp', 'ep', 'tp')), parts along dimension 0
There are 4 independent parts, one for each index of `grp`. A program takes and returns all parts, laid end to end along the dimension named above; an argument that names none is the same for every part. Nothing has to cross between parts.
Inputs may be any that keep to these rules, and one draw needn't show every extreme that they name: `expert_ids`: each token names 4 different experts. Among the 128 tokens of one device (aligned blocks of rows) no expert is named more than 16 times, a bound that some block reaches.
All inputs are finite; a program needn't handle non-finite values.
Results may differ from a plain program's by a relative error of at most 0.0071.
Values may be sent and summed in bfloat16 or wider, within the bound.
A program may use at most 64 MiB of HBM per device.

v0:
```python
import jax
import jax.numpy as jnp
from jax import lax
from jax.sharding import PartitionSpec as P

norm_eps = 1e-05
clamp_limit = 7.0
sig_alpha = 1.702


def layer_norm(tokens, norm_gain):
    values = tokens.astype(jnp.float32)
    row_mean = jnp.mean(values, -1, keepdims=True)
    centred = values - row_mean
    row_var = jnp.mean(centred * centred, -1, keepdims=True)
    scaled = centred * lax.rsqrt(row_var + norm_eps) * norm_gain
    return scaled.astype(jnp.bfloat16)


def expert_apply(inputs, gate_mat, up_mat, down_mat):
    gate_pre = jnp.dot(inputs, gate_mat, preferred_element_type=jnp.float32)
    up_pre = jnp.dot(inputs, up_mat, preferred_element_type=jnp.float32)
    gated = jnp.minimum(gate_pre, clamp_limit)
    upper = jnp.clip(up_pre, -clamp_limit, clamp_limit)
    hidden = (gated * jax.nn.sigmoid(sig_alpha * gated) * (upper + 1.0)).astype(jnp.bfloat16)
    return jnp.dot(hidden, down_mat, preferred_element_type=jnp.float32).astype(jnp.bfloat16)


def local(tokens, expert_ids, route_weights, norm_gain, w_gate, w_up, w_down):
    ep_count = lax.axis_size("ep")
    tp_count = lax.axis_size("tp")
    experts = ep_count * tp_count
    tok_rows, feat_width = tokens.shape
    top_count = expert_ids.shape[1]
    capacity = 2 * tok_rows * top_count // experts
    normed = layer_norm(tokens, norm_gain)
    flat_ids = expert_ids.reshape(-1)
    one_hot = (flat_ids[:, None] == jnp.arange(experts, dtype=jnp.int32)[None, :]).astype(jnp.int32)
    slot_index = jnp.sum((jnp.cumsum(one_hot, 0) - one_hot) * one_hot, 1)
    target = flat_ids * capacity + slot_index
    pair_token = jnp.arange(tok_rows * top_count, dtype=jnp.int32) // top_count
    buffer = (
        jnp.zeros((experts * capacity, feat_width), jnp.bfloat16).at[target].set(normed[pair_token])
    )
    buffer = buffer.reshape(experts, capacity, feat_width)
    gate_mat = w_gate[0]
    up_mat = w_up[0]
    down_mat = w_down[0]
    arrived = lax.all_to_all(buffer, ("ep", "tp"), split_axis=0, concat_axis=0, tiled=True)
    flat_rows = arrived.reshape(-1, feat_width)
    returned = lax.all_to_all(
        expert_apply(flat_rows, gate_mat, up_mat, down_mat).reshape(arrived.shape),
        ("ep", "tp"),
        split_axis=0,
        concat_axis=0,
        tiled=True,
    )
    picked = returned.reshape(experts * capacity, feat_width)[target].reshape(
        tok_rows, top_count, feat_width
    )
    combined = jnp.zeros((tok_rows, feat_width), jnp.float32)
    for choice_slot in range(top_count):
        combined = combined + route_weights[:, choice_slot : choice_slot + 1] * picked[
            :, choice_slot
        ].astype(jnp.float32)
    return combined.astype(jnp.bfloat16)


def solution(mesh):
    placed = (
        P(("grp", "ep", "tp"), None),
        P(("grp", "ep", "tp"), None),
        P(("grp", "ep", "tp"), None),
        P(),
        P(("ep", "tp"), None, None),
        P(("ep", "tp"), None, None),
        P(("ep", "tp"), None, None),
    )
    return jax.shard_map(
        local, mesh=mesh, in_specs=placed, out_specs=P(("grp", "ep", "tp"), None), check_vma=False
    )
```

profile of v0, /device:TPU:37, one launch (start us, length us, event | category | flops | bytes accessed | tf_op | source)
XLA Modules:
  0.0 853.5 jit_solution(11359488160024532716)
XLA Ops:
  0.0 0.8 copy.13
  0.8 0.1 eq.29
  0.9 0.1 eq.25
  1.0 0.7 broadcast_multiply_fusion
  1.7 1.2 reduce-window.6
  2.9 0.2 slice_reduce_fusion
  3.2 0.1 copy.12
  3.3 0.1 mul.94
  3.4 1.2 convert_reduce_fusion
  4.6 1.3 fusion.12
  6.0 0.1 fusion.21
  6.1 1.4 fusion.14
  7.5 12.8 %scatter_custom_fusion = bf16[1024,2048]{1,0:T(8,128)(2,1)} fusion(s32[512]{0:T(512)S(1)} %bitcast.73, bf16[128,2048]{1,0:T(8,128)(2,1)S(1)} %fusion.14, s32[1024]{0:T(1024)S(1)} %pad_clamp_fusion.1, bf16[]{:T(256)} %constant.15.clone.1), kind=kCustom, calls=%fused_computation.10 | custom fusion | bytes 4194306 | tf_op jit(solution)/shard_map/scatter | solution.py:43
  20.3 0.0 copy-start.1
  20.3 411.7 %all_to_all.10 = bf16[64,16,2048]{2,1,0:T(8,128)(2,1)S(1)} all-to-all(bf16[64,16,2048]{2,1,0:T(8,128)(2,1)} %bitcast.68), channel_id=1, replica_groups=mesh['grp'=4,'ep'=32,'tp'=2] {'ep','tp'}, dimensions={0} | all-to-all | bytes 8388608 | tf_op jit(solution)/shard_map/all_to_all | solution.py:49
  432.1 0.0 copy-done.1
  432.1 0.0 copy-start.2
  432.1 4.5 fusion.1
  436.6 0.0 copy-done.2
  436.6 0.0 copy-start.3
  436.6 5.1 multiply_convert_fusion
  441.7 0.0 copy-done.3
  441.8 6.1 convolution_convert_fusion
  447.8 0.0 copy-start
  447.8 8.8 %all-to-all-start.1 = ((bf16[64,16,2048]{2,1,0:T(8,128)(2,1)}), bf16[64,16,2048]{2,1,0:T(8,128)(2,1)}, u32[]{:S(2)}, u32[]{:S(2)}) async-start(bf16[64,16,2048]{2,1,0:T(8,128)(2,1)} %bitcast.69), calls=%async_computation.1 | async-start | bytes 8388608 | tf_op jit(solution)/shard_map/all_to_all | solution.py:51
  456.6 0.0 copy-done
  456.6 380.1 %all-to-all-done.1 = bf16[64,16,2048]{2,1,0:T(8,128)(2,1)} async-done(((bf16[64,16,2048]{2,1,0:T(8,128)(2,1)}), bf16[64,16,2048]{2,1,0:T(8,128)(2,1)}, u32[]{:S(2)}, u32[]{:S(2)}) %all-to-all-start.1) | async-done | bytes 4194336 | tf_op jit(solution)/shard_map/all_to_all | solution.py:51
  836.7 8.0 gather_fusion
  844.7 2.7 reshape.130
  847.4 3.1 fusion.23
  850.5 3.0 fusion.16
  (10 shorter events, 0.1 us)
Async XLA Ops:
  20.3 411.7 %copy-start.1 = (bf16[1,2048,896]{2,1,0:T(8,128)(2,1)S(1)}, bf16[1,2048,896]{2,1,0:T(8,128)(2,1)}, u32[]{:S(2)}) copy-start(bf16[1,2048,896]{2,1,0:T(8,128)(2,1)} %param.12) | copy-start | bytes 11010052
  432.1 4.5 copy-start.2
  436.6 5.2 copy-start.3
  447.8 8.8 %copy-start = (f32[128,4]{0,1:T(4,128)S(1)}, f32[128,4]{0,1:T(4,128)}, u32[]{:S(2)}) copy-start(f32[128,4]{0,1:T(4,128)} %param.9) | copy-start | bytes 6148
  447.8 388.9 %all-to-all-start.1 = ((bf16[64,16,2048]{2,1,0:T(8,128)(2,1)}), bf16[64,16,2048]{2,1,0:T(8,128)(2,1)}, u32[]{:S(2)}, u32[]{:S(2)}) async-start(bf16[64,16,2048]{2,1,0:T(8,128)(2,1)} %bitcast.69), calls=%async_computation.1 | async-start | bytes 8388608 | tf_op jit(solution)/shard_map/all_to_all | solution.py:51
where the time goes:
time: 854 us
  blocking collectives  412 us (48%)
  waiting for transfers between devices  380 us (44%)
  local copies, waits for them, and re-layouts  28.1 us (3%)
  matrix products  15.7 us (2%)
  other arithmetic  9.02 us (1%)
  starting transfers between devices  8.77 us (1%)
    all_to_all x1, blocking collectives, local(): lax.all_to_all(buffer, ('ep', 'tp'), split_axis=0, concat_axis=0, tiled=T...  412 us
    all_to_all x1, waiting for transfers between devices, local(): lax.all_to_all(expert_apply(flat_rows, gate_mat, up_mat, down_mat).reshap...  380 us
  transfers between devices with their start and end apart: 1, of which 1 were waited for; matrix products, arithmetic and copies ran while one was open for 0% of the time, Pallas kernels for 0%

commit v1 on v0

v1 whole, which is shorter than its diff:
```python
import functools

import jax
import jax.numpy as jnp
from jax import lax
from jax.experimental import pallas as pl
from jax.experimental.pallas import tpu as pltpu
from jax.sharding import PartitionSpec as P

norm_eps = 1e-05
clamp_limit = 7.0
sig_alpha = 1.702

F32 = jnp.float32
BF16 = jnp.bfloat16
VMEM_BYTES = 67_043_328


def iota(shape, dim):
    return lax.broadcasted_iota(jnp.int32, shape, dim)


def dot(a, b):
    return jnp.dot(a, b, preferred_element_type=F32)


def routed_kernel(
    cap,
    tokens_ref, ids_ref, gates_ref, gain_ref, wg_hbm, wu_hbm, wd_hbm,
    out_ref,
    wgu, wd, xn, unsort,
    ag0, ag1, rs0, rs1, md0, md1, st0, st1,
    xin, xout, yy, yout,
    w_sem, ag_rv0, ag_rv1, rs_rv0, rs_rv1, md_rv0, md_rv1, x_rv, y_rv,
    ag_tx, rs_tx, md_tx, x_tx, y_tx,
):
    n = lax.axis_size("ep")
    cores = lax.axis_size("tp")
    me = lax.axis_index("ep")
    core = lax.axis_index("tp")
    rows, width = tokens_ref.shape
    top = ids_ref.shape[0]
    hidden_width = wg_hbm.shape[2]
    experts = n * cores
    quad = cores * cap
    parts = rows // quad
    reach = (n // 2, n - 1 - n // 2)
    batch = 2 * quad
    ag, rs, md, st = (ag0, ag1), (rs0, rs1), (md0, md1), (st0, st1)
    ag_rv, rs_rv, md_rv = (ag_rv0, ag_rv1), (rs_rv0, rs_rv1), (md_rv0, md_rv1)

    turn = 1 - 2 * core
    nxt = (lax.rem(me + turn + n, n), lax.rem(me - turn + n, n))
    partner = {"tp": 1 - core}

    def copy_to(src, dst, tx, rv, device):
        return pltpu.make_async_remote_copy(
            src_ref=src, dst_ref=dst, send_sem=tx, recv_sem=rv,
            device_id=device, device_id_type=pl.DeviceIdType.MESH,
        )

    loads = (
        pltpu.make_async_copy(wg_hbm.at[0], wgu.at[:, pl.ds(0, hidden_width)], w_sem.at[0]),
        pltpu.make_async_copy(wu_hbm.at[0], wgu.at[:, pl.ds(hidden_width, hidden_width)], w_sem.at[1]),
        pltpu.make_async_copy(wd_hbm.at[0], wd, w_sem.at[2]),
    )
    for load in loads:
        load.start()

    barrier = pltpu.get_barrier_semaphore()
    for device in ({"ep": nxt[0]}, {"ep": nxt[1]}, partner):
        pl.semaphore_signal(barrier, inc=1, device_id=device, device_id_type=pl.DeviceIdType.MESH)

    def norm_rows(g, carry):
        at = pl.ds(pl.multiple_of(g * 16, 16), 16)
        values = tokens_ref[at, :].astype(F32)
        centred = values - jnp.mean(values, -1, keepdims=True)
        var = jnp.mean(centred * centred, -1, keepdims=True)
        xn[at, :] = (centred * lax.rsqrt(var + norm_eps) * gain_ref[...]).astype(BF16)
        return carry

    lax.fori_loop(0, rows // 16, norm_rows, 0)

    ids = ids_ref[...]
    lane = iota((1, rows), 1)
    hits = [ids[k:k + 1] == iota((experts, rows), 0) for k in range(top)]
    named = functools.reduce(jnp.add, [h.astype(F32) for h in hits])
    earlier = (iota((rows, rows), 0) < iota((rows, rows), 1)).astype(BF16)
    before = dot(named.astype(BF16), earlier)
    slots = [jnp.sum(jnp.where(h, before, 0.0), 0, keepdims=True) for h in hits]
    codes = [(cap * ids[k:k + 1]).astype(F32) + slots[k] for k in range(top)]
    meta = jnp.concatenate(codes + [gates_ref[k:k + 1] for k in range(top)], 0)
    meta_hi = meta.astype(BF16)
    rest = meta - meta_hi.astype(F32)
    meta_mid = rest.astype(BF16)
    meta_lo = (rest - meta_mid.astype(F32)).astype(BF16)

    away = lax.rem((ids // cores - me) * turn + 2 * n, n)
    eye = iota((rows, rows), 0) == iota((rows, rows), 1)
    place = []
    for d in range(2):
        far = away if d == 0 else n - away
        inside = (away <= reach[0]) if d == 0 else (away > reach[0])
        far = jnp.max(jnp.where(inside, far, 0), 0, keepdims=True)
        key = (far * rows + (rows - 1 - lane)).astype(F32)
        key_col = jnp.sum(jnp.where(eye, key, 0.0), 1, keepdims=True)
        rank = jnp.sum((key_col > key).astype(F32), 0, keepdims=True)
        rank_col = jnp.sum((key > key_col).astype(F32), 1, keepdims=True)
        place.append((iota((rows, rows), 0).astype(F32) == rank).astype(BF16))
        back = (iota((rows, rows), 1).astype(F32) == rank_col).astype(BF16)
        unsort[d] = back
        md[d][0:8, :] = dot(meta_hi, back) + dot(meta_mid, back) + dot(meta_lo, back)

    def sort_part(i):
        for d in range(2):
            ag[d][quad * i:quad * (i + 1), :] = dot(
                place[d][quad * i:quad * (i + 1)], xn[...]
            ).astype(BF16)

    for d in range(2):
        for short in range(1, parts):
            h = reach[d] - parts + 1 + short
            top_row = rows * h + quad * (parts - short)
            ag[d][top_row:rows * (h + 1), :] = jnp.zeros((quad * short, width), BF16)
    for j in (0, reach[0]):
        xin[batch * j + cap:batch * j + 2 * cap, :] = jnp.zeros((cap, width), BF16)
        xout[quad * j + cap:quad * (j + 1), :] = jnp.zeros((cap, width), BF16)

    def send_part(d, i, h):
        at = pl.multiple_of(rows * (h - 1) + quad * i, quad)
        if i == 0:
            m = pl.multiple_of(8 * (h - 1), 8)
            copy_to(md[d].at[pl.ds(m, 8)], md[d].at[pl.ds(m + 8, 8)],
                    md_tx.at[d], md_rv[d].at[h], {"ep": nxt[d]}).start()
        copy_to(ag[d].at[pl.ds(at, quad)], ag[d].at[pl.ds(at + rows, quad)],
                ag_tx.at[d], ag_rv[d].at[h, i], {"ep": nxt[d]}).start()

    def take_part(d, i, h):
        at = pl.multiple_of(rows * h + quad * i, quad)
        if i == 0:
            m = md[d].at[pl.ds(pl.multiple_of(8 * h, 8), 8)]
            copy_to(m, m, md_tx.at[d], md_rv[d].at[h], {"ep": nxt[d]}).wait_recv()
        part = ag[d].at[pl.ds(at, quad)]
        copy_to(part, part, ag_tx.at[d], ag_rv[d].at[h, i], {"ep": nxt[d]}).wait_recv()

    def select_rows(d, j, meta, block):
        row = iota((quad, rows), 0)
        want = (quad * me + lax.rem(cap * core + row, quad)).astype(F32)
        pick = jnp.zeros((quad, rows), F32)
        weight = jnp.zeros((quad, rows), F32)
        for k in range(top):
            hit = meta[k:k + 1] == want
            pick = jnp.where(hit, 1.0, pick)
            weight = jnp.where(hit, meta[top + k:top + k + 1], weight)
        found = dot(pick.astype(BF16), block).astype(BF16)
        xin[pl.ds(pl.multiple_of(batch * j + cap * d, cap), cap), :] = found[:cap]
        xout[pl.ds(pl.multiple_of(quad * j + cap * d, cap), cap), :] = found[cap:]
        none = jnp.zeros((cap, rows), F32)
        mine, other = weight[:cap], weight[cap:]
        spread = (mine, none, other, none) if d == 0 else (none, mine, none, other)
        spread = jnp.concatenate(spread + (jnp.zeros((rows - batch, rows), F32),), 0)
        st[d][pl.ds(pl.multiple_of(rows * j, rows), rows), :] = spread.T.astype(BF16)

    def select_block(d, j):
        at = pl.multiple_of(rows * j, rows)
        select_rows(d, j, md[d][pl.ds(pl.multiple_of(8 * j, 8), 8), :], ag[d][pl.ds(at, rows), :])

    def x_copy(j):
        return copy_to(xout.at[pl.ds(pl.multiple_of(quad * j, quad), quad)],
                       xin.at[pl.ds(pl.multiple_of(batch * j + quad, quad), quad)],
                       x_tx, x_rv.at[j], partner)

    def y_copy(j):
        return copy_to(yout.at[pl.ds(pl.multiple_of(quad * j, quad), quad)],
                       yy.at[pl.ds(pl.multiple_of(batch * j + quad, quad), quad)],
                       y_tx, y_rv.at[j], partner)

    def expert_batch(j):
        x_copy(j).wait_recv()
        at = pl.multiple_of(batch * j, batch)
        pre = dot(xin[pl.ds(at, batch), :], wgu[...])
        gated = jnp.minimum(pre[:, :hidden_width], clamp_limit)
        upper = jnp.clip(pre[:, hidden_width:], -clamp_limit, clamp_limit)
        hidden = (gated * jax.nn.sigmoid(sig_alpha * gated) * (upper + 1.0)).astype(BF16)
        result = dot(hidden, wd[...]).astype(BF16)
        yy[pl.ds(at, quad), :] = result[:quad]
        yout[pl.ds(pl.multiple_of(quad * j, quad), quad), :] = result[quad:]
        y_copy(j).start()

    sort_part(0)
    pl.semaphore_wait(barrier, 3)
    both = (0, 1)
    for d in both:
        send_part(d, 0, 1)
    sort_part(1)
    for d in both:
        send_part(d, 1, 1)
    sort_part(2)
    sort_part(3)
    for d in both:
        take_part(d, 0, 1)
        send_part(d, 0, 2)
    select_rows(0, 0, meta, xn[...])
    x_copy(0).start()
    for d in both:
        take_part(d, 1, 1)
        send_part(d, 1, 2)
    for d in both:
        take_part(d, 0, 2)
        send_part(d, 0, 3)
    for d in both:
        send_part(d, 2, 1)
    for i in range(3):
        for d in both:
            take_part(d, i, 3 - i)
            send_part(d, i, 4 - i)
    for d in both:
        send_part(d, 3, 1)
    for load in loads:
        load.wait()

    def round_of(r, moving):
        for i in range(parts):
            h = r + 2 - i
            for d in both:
                take_part(d, i, h)
                if d in moving:
                    send_part(d, i, h + 1)
            if i == 0:
                expert_batch(r - 2)
        for d in both:
            select_block(d, r - 1)
        x_copy(r - 1).start()

    def round_body(r, carry):
        round_of(r, both)
        return carry

    last = reach[1] - parts + 1
    lax.fori_loop(2, last + 1, round_body, 0)
    round_of(last + 1, (0,))
    for j in range(last + 1, reach[1] + 1):
        select_block(1, j)
    expert_batch(last)
    for i in range(parts):
        take_part(0, i, reach[0] - i)
        select_block(0, reach[0] - i)
        x_copy(reach[0] - i).start()

    def y_wait(j):
        y_copy(j).wait_recv()

    def give_part(d, j, i, fresh=False):
        at = pl.multiple_of(rows * j + quad * i, quad)
        share = dot(st[d][pl.ds(at, quad), :][:, :batch], yy[pl.ds(pl.multiple_of(batch * j, batch), batch), :])
        part = rs[d].at[pl.ds(at, quad)]
        if not fresh:
            copy_to(part, part, rs_tx.at[d], rs_rv[d].at[j, i], {"ep": nxt[d]}).wait_recv()
            share = share + part[...].astype(F32)
        part[...] = share.astype(BF16)
        copy_to(part, rs[d].at[pl.ds(at - rows, quad)], rs_tx.at[d], rs_rv[d].at[j - 1, i],
                {"ep": nxt[1 - d]}).start()

    def y_wait_body(j, carry):
        y_wait(j)
        return carry

    lax.fori_loop(0, last + 1, y_wait_body, 0)
    give_part(1, last, parts - 1, True)

    def turn_body(t, carry):
        expert_batch(reach[0] - t)

        @pl.when(t >= 1)
        def _():
            y_wait(reach[0] + 1 - t)
            give_part(0, reach[0] + 1 - t, t - 1, True)

        @pl.when(t >= 2)
        def _():
            give_part(1, reach[0] + 1 - t, t - 2, True)

        return carry

    lax.fori_loop(0, parts, turn_body, 0)
    y_wait(last + 1)
    give_part(0, last + 1, parts - 1, True)
    give_part(1, last + 1, parts - 2, True)

    def give_body(r, carry):
        for i in range(parts):
            for d in both:
                give_part(d, reach[d] - i - r, i)
        return carry

    lax.fori_loop(1, last, give_body, 0)
    closing = ((3, 0), (2, 1), (1, 2), (2, 0), (1, 1), (1, 0))
    order0 = tuple((parts - i, i) for i in range(parts)) + closing
    for step in range(len(order0)):
        give_part(0, *order0[step])
        if step < len(closing):
            give_part(1, *closing[step])

    for d in both:
        for i in range(parts):
            part = rs[d].at[pl.ds(quad * i, quad)]
            copy_to(part, part, rs_tx.at[d], rs_rv[d].at[0, i], {"ep": nxt[d]}).wait_recv()
    mixed = dot(st0[0:rows, :][:, :batch], yy[0:batch, :])
    for d in both:
        mixed = mixed + dot(unsort[d], rs[d][0:rows, :])
    out_ref[...] = mixed.astype(BF16)

    for d in both:
        moved = quad * sum(reach[d] - i for i in range(parts))
        sent = ag[d].at[pl.ds(0, moved)]
        copy_to(sent, sent, ag_tx.at[d], ag_rv[d].at[0, 0], {"ep": nxt[d]}).wait_send()
        sent = rs[d].at[pl.ds(0, moved)]
        copy_to(sent, sent, rs_tx.at[d], rs_rv[d].at[0, 0], {"ep": nxt[d]}).wait_send()
        sent = md[d].at[pl.ds(0, 8 * reach[d])]
        copy_to(sent, sent, md_tx.at[d], md_rv[d].at[0], {"ep": nxt[d]}).wait_send()
    copy_to(xout, xout, x_tx, x_rv.at[0], partner).wait_send()
    copy_to(yout, yout, y_tx, y_rv.at[0], partner).wait_send()


def local(tokens, expert_ids, route_weights, norm_gain, w_gate, w_up, w_down):
    n = lax.axis_size("ep")
    cores = lax.axis_size("tp")
    rows, width = tokens.shape
    top = expert_ids.shape[1]
    hidden_width = w_gate.shape[2]
    cap = 2 * rows * top // (n * cores)
    quad = cores * cap
    parts = rows // quad
    reach = (n // 2, n - 1 - n // 2)
    batches = reach[0] + 1
    vmem = pl.BlockSpec(memory_space=pltpu.VMEM)
    hbm = pl.BlockSpec(memory_space=pl.ANY)
    dma = pltpu.SemaphoreType.DMA
    blocks = [pltpu.VMEM((rows * (r + 1), width), BF16) for r in reach]
    return pl.pallas_call(
        functools.partial(routed_kernel, cap),
        name="routed_layer",
        out_shape=jax.ShapeDtypeStruct((rows, width), BF16),
        in_specs=[vmem] * 4 + [hbm] * 3,
        out_specs=vmem,
        scratch_shapes=[
            pltpu.VMEM((width, 2 * hidden_width), BF16),
            pltpu.VMEM((hidden_width, width), BF16),
            pltpu.VMEM((rows, width), BF16),
            pltpu.VMEM((2, rows, rows), BF16),
            *blocks,
            *blocks,
            *[pltpu.VMEM((8 * (r + 1), rows), F32) for r in reach],
            *[pltpu.VMEM((rows * (r + 1), rows), BF16) for r in reach],
            pltpu.VMEM((2 * quad * batches, width), BF16),
            pltpu.VMEM((quad * batches, width), BF16),
            pltpu.VMEM((2 * quad * batches, width), BF16),
            pltpu.VMEM((quad * batches, width), BF16),
            dma((3,)),
            *[dma((r + 1, parts)) for r in reach],
            *[dma((r + 1, parts)) for r in reach],
            *[dma((r + 1,)) for r in reach],
            dma((batches,)),
            dma((batches,)),
            dma((2,)),
            dma((2,)),
            dma((2,)),
            dma,
            dma,
        ],
        compiler_params=pltpu.CompilerParams(
            collective_id=0, has_side_effects=True, vmem_limit_bytes=VMEM_BYTES
        ),
    )(tokens, expert_ids.T, route_weights.T, norm_gain.reshape(1, width), w_gate, w_up, w_down)


def solution(mesh):
    placed = (
        P(("grp", "ep", "tp"), None),
        P(("grp", "ep", "tp"), None),
        P(("grp", "ep", "tp"), None),
        P(),
        P(("ep", "tp"), None, None),
        P(("ep", "tp"), None, None),
        P(("ep", "tp"), None, None),
    )
    return jax.shard_map(
        local, mesh=mesh, in_specs=placed, out_specs=P(("grp", "ep", "tp"), None), check_vma=False
    )
```

time: 854 us -> 358 us (0.42)
  blocking collectives: 412 us -> 0 us
  waiting for transfers between devices: 380 us -> 0 us
  Pallas kernels: 0 us -> 356 us
  local copies, waits for them, and re-layouts: 28.1 us -> 1.88 us
  matrix products: 15.7 us -> 0 us
  other arithmetic: 9.02 us -> 0 us
  starting transfers between devices: 8.77 us -> 0 us
    all_to_all x1 -> x0, blocking collectives: 412 us -> none  [local(): lax.all_to_all(buffer, ('ep', 'tp'), split_axis=0, concat_axis=0, tiled=T...]
    all_to_all x1 -> x0, waiting for transfers between devices: 380 us -> none  [local(): lax.all_to_all(expert_apply(flat_rows, gate_mat, up_mat, down_mat).reshap...]
    pallas_call x0 -> x1, Pallas kernels: none -> 356 us  [local(): pl.pallas_call(functools.partial(routed_kernel, cap), name='routed_layer'...]
    dot_general x3 -> x0, matrix products: 15.7 us -> none  [the longest x1 6.07 us: expert_apply(): jnp.dot(hidden, down_mat, preferred_element_type=jnp.float32)]
    scatter x1 -> x0, local copies, waits for them, and re-layouts: 12.8 us -> none  [local(): jnp.zeros((experts * capacity, feat_width), jnp.bfloat16).at[target]]
    all_to_all x1 -> x0, starting transfers between devices: 8.77 us -> none  [local(): lax.all_to_all(expert_apply(flat_rows, gate_mat, up_mat, down_mat).reshap...]
  transfers between devices with their start and end apart: 1 -> 0, of which waited for: 1 -> 0; matrix products, arithmetic and copies ran while one was open for 0% -> 0% of each run, Pallas kernels for 0% -> 0%
where the time goes in v1:
time: 358 us
  Pallas kernels  356 us (99%)
    pallas_call x1, Pallas kernels, local(): pl.pallas_call(functools.partial(routed_kernel, cap), name='routed_layer'...  356 us

profile of v1, /device:TPU:37, one launch (start us, length us, event | category | flops | bytes accessed | tf_op | source)
XLA Modules:
  0.0 357.6 jit_solution(7454083229325780604)
XLA Ops:
  0.0 355.7 %routed_layer.1 = bf16[128,2048]{1,0:T(8,128)(2,1)} custom-call(bf16[128,2048]{1,0:T(8,128)(2,1)} %tokens_ref.1, s32[4,128]{1,0:T(4,128)} %bitcast.4, f32[4,128]{1,0:T(4,128)} %bitcast.5, f32[1,2048]{1,0:T(1,128)} %bitcast.3, bf16[1,2048,896]{2,1,0:T(8,128)(2,1)} %wg_hbm.1, bf16[1,2048,896]{2,1,0:T(8,128)(2,1)} %wu_hbm.1, bf16[1,896,2048]{2,1,0:T(8,128)(2,1)} %wd_hbm.1), custom_call_target="tpu_custom_call" | custom-call | tf_op jit(solution)/shard_map/routed_layer/pallas_call | solution.py:340
  355.8 1.9 copy.9

commit v2 on v1

v2 whole, which is shorter than its diff:
```python
import functools

import jax
import jax.numpy as jnp
from jax import lax
from jax.experimental import pallas as pl
from jax.experimental.pallas import tpu as pltpu
from jax.sharding import PartitionSpec as P

norm_eps = 1e-05
clamp_limit = 7.0
sig_alpha = 1.702

F32 = jnp.float32
BF16 = jnp.bfloat16
VMEM_BYTES = 67_043_328


def iota(shape, dim):
    return lax.broadcasted_iota(jnp.int32, shape, dim)


def dot(a, b):
    return jnp.dot(a, b, preferred_element_type=F32)


def routed_kernel(
    cap,
    ids_ref, gates_ref, gain_ref, tokens_hbm, wg_hbm, wu_hbm, wd_hbm,
    out_ref,
    tokens, wgu, wd, unsort, total,
    ag0, ag1, rs0, rs1, md0, md1, st0, st1,
    xin, xout, yy, yout,
    w_sem, ag_rv0, ag_rv1, rs_rv0, rs_rv1, md_rv0, md_rv1, x_rv, y_rv,
    ag_tx, rs_tx, md_tx, x_tx, y_tx,
):
    n = lax.axis_size("ep")
    cores = lax.axis_size("tp")
    me = lax.axis_index("ep")
    core = lax.axis_index("tp")
    rows, width = tokens_hbm.shape
    top = ids_ref.shape[0]
    hidden_width = wg_hbm.shape[2]
    experts = n * cores
    quad = cores * cap
    parts = rows // quad
    reach = (n // 2, n - 1 - n // 2)
    both = (0, 1)
    batch = 2 * quad
    ag, rs, md, st = (ag0, ag1), (rs0, rs1), (md0, md1), (st0, st1)
    ag_rv, rs_rv, md_rv = (ag_rv0, ag_rv1), (rs_rv0, rs_rv1), (md_rv0, md_rv1)

    turn = 1 - 2 * core
    nxt = (lax.rem(me + turn + n, n), lax.rem(me - turn + n, n))
    partner = {"tp": 1 - core}

    def copy_to(src, dst, tx, rv, device):
        return pltpu.make_async_remote_copy(
            src_ref=src, dst_ref=dst, send_sem=tx, recv_sem=rv,
            device_id=device, device_id_type=pl.DeviceIdType.MESH,
        )

    token_load = pltpu.make_async_copy(tokens_hbm, tokens, w_sem.at[3])
    token_load.start()
    loads = (
        pltpu.make_async_copy(wg_hbm.at[0], wgu.at[:, pl.ds(0, hidden_width)], w_sem.at[0]),
        pltpu.make_async_copy(wu_hbm.at[0], wgu.at[:, pl.ds(hidden_width, hidden_width)], w_sem.at[1]),
        pltpu.make_async_copy(wd_hbm.at[0], wd, w_sem.at[2]),
    )
    for load in loads:
        load.start()

    barrier = pltpu.get_barrier_semaphore()
    for device in ({"ep": nxt[0]}, {"ep": nxt[1]}, partner):
        pl.semaphore_signal(barrier, inc=1, device_id=device, device_id_type=pl.DeviceIdType.MESH)

    ids = ids_ref[...]
    lane = iota((1, rows), 1)
    hits = [ids[k:k + 1] == iota((experts, rows), 0) for k in range(top)]
    named = functools.reduce(jnp.add, [h.astype(F32) for h in hits])
    earlier = (iota((rows, rows), 0) < iota((rows, rows), 1)).astype(BF16)
    before = dot(named.astype(BF16), earlier)
    slots = [jnp.sum(jnp.where(h, before, 0.0), 0, keepdims=True) for h in hits]
    codes = [(cap * ids[k:k + 1]).astype(F32) + slots[k] for k in range(top)]
    meta = jnp.concatenate(codes + [gates_ref[k:k + 1] for k in range(top)], 0)
    meta_hi = meta.astype(BF16)
    rest = meta - meta_hi.astype(F32)
    meta_mid = rest.astype(BF16)
    meta_lo = (rest - meta_mid.astype(F32)).astype(BF16)

    away = lax.rem((ids // cores - me) * turn + 2 * n, n)
    eye = iota((rows, rows), 0) == iota((rows, rows), 1)
    place = []
    for d in range(2):
        far = away if d == 0 else n - away
        inside = (away <= reach[0]) if d == 0 else (away > reach[0])
        far = jnp.max(jnp.where(inside, far, 0), 0, keepdims=True)
        key = (far * rows + (rows - 1 - lane)).astype(F32)
        key_col = jnp.sum(jnp.where(eye, key, 0.0), 1, keepdims=True)
        rank = jnp.sum((key_col > key).astype(F32), 0, keepdims=True)
        rank_col = jnp.sum((key > key_col).astype(F32), 1, keepdims=True)
        place.append((iota((rows, rows), 0).astype(F32) == rank).astype(BF16))
        back = (iota((rows, rows), 1).astype(F32) == rank_col).astype(BF16)
        unsort[d] = back
        md[d][0:8, :] = dot(meta_hi, back) + dot(meta_mid, back) + dot(meta_lo, back)

    def sort_part(d, i):
        at = slice(quad * i, quad * (i + 1))
        values = dot(place[d][at], tokens[...])
        centred = values - jnp.mean(values, -1, keepdims=True)
        var = jnp.mean(centred * centred, -1, keepdims=True)
        ag[d][at, :] = (centred * lax.rsqrt(var + norm_eps) * gain_ref[...]).astype(BF16)

    def blank_rows():
        for d in range(2):
            for short in range(1, parts):
                h = reach[d] - parts + 1 + short
                top_row = rows * h + quad * (parts - short)
                ag[d][top_row:rows * (h + 1), :] = jnp.zeros((quad * short, width), BF16)

    def send_part(d, i, h):
        at = pl.multiple_of(rows * (h - 1) + quad * i, quad)
        if i == 0:
            m = pl.multiple_of(8 * (h - 1), 8)
            copy_to(md[d].at[pl.ds(m, 8)], md[d].at[pl.ds(m + 8, 8)],
                    md_tx.at[d], md_rv[d].at[h], {"ep": nxt[d]}).start()
        copy_to(ag[d].at[pl.ds(at, quad)], ag[d].at[pl.ds(at + rows, quad)],
                ag_tx.at[d], ag_rv[d].at[h, i], {"ep": nxt[d]}).start()

    def take_part(d, i, h):
        at = pl.multiple_of(rows * h + quad * i, quad)
        if i == 0:
            m = md[d].at[pl.ds(pl.multiple_of(8 * h, 8), 8)]
            copy_to(m, m, md_tx.at[d], md_rv[d].at[h], {"ep": nxt[d]}).wait_recv()
        part = ag[d].at[pl.ds(at, quad)]
        copy_to(part, part, ag_tx.at[d], ag_rv[d].at[h, i], {"ep": nxt[d]}).wait_recv()

    def select_block(d, b):
        j = b - d
        meta = md[d][pl.ds(pl.multiple_of(8 * j, 8), 8), :]
        row = iota((quad, rows), 0)
        want = (quad * me + lax.rem(cap * core + row, quad)).astype(F32)
        pick = jnp.zeros((quad, rows), F32)
        weight = jnp.zeros((quad, rows), F32)
        for k in range(top):
            hit = meta[k:k + 1] == want
            pick = jnp.where(hit, 1.0, pick)
            weight = jnp.where(hit, meta[top + k:top + k + 1], weight)
        block = ag[d][pl.ds(pl.multiple_of(rows * j, rows), rows), :]
        found = dot(pick.astype(BF16), block).astype(BF16)
        xin[pl.ds(pl.multiple_of(batch * (b - 1) + cap * d, cap), cap), :] = found[:cap]
        xout[pl.ds(pl.multiple_of(quad * (b - 1) + cap * d, cap), cap), :] = found[cap:]
        none = jnp.zeros((cap, rows), F32)
        mine, other = weight[:cap], weight[cap:]
        spread = (mine, none, other, none) if d == 0 else (none, mine, none, other)
        spread = jnp.concatenate(spread + (jnp.zeros((rows - batch, rows), F32),), 0)
        st[d][pl.ds(pl.multiple_of(rows * j, rows), rows), :] = spread.T.astype(BF16)

    def select_batch(b):
        for d in both:
            select_block(d, b)
        x_copy(b).start()

    def x_copy(b):
        return copy_to(xout.at[pl.ds(pl.multiple_of(quad * (b - 1), quad), quad)],
                       xin.at[pl.ds(pl.multiple_of(batch * (b - 1) + quad, quad), quad)],
                       x_tx, x_rv.at[b - 1], partner)

    def y_copy(b):
        return copy_to(yout.at[pl.ds(pl.multiple_of(quad * (b - 1), quad), quad)],
                       yy.at[pl.ds(pl.multiple_of(batch * (b - 1) + quad, quad), quad)],
                       y_tx, y_rv.at[b - 1], partner)

    def expert_batch(b):
        x_copy(b).wait_recv()
        at = pl.multiple_of(batch * (b - 1), batch)
        pre = dot(xin[pl.ds(at, batch), :], wgu[...])
        gated = jnp.minimum(pre[:, :hidden_width], clamp_limit)
        upper = jnp.clip(pre[:, hidden_width:], -clamp_limit, clamp_limit)
        hidden = (gated * jax.nn.sigmoid(sig_alpha * gated) * (upper + 1.0)).astype(BF16)
        result = dot(hidden, wd[...]).astype(BF16)
        yy[pl.ds(at, quad), :] = result[:quad]
        yout[pl.ds(pl.multiple_of(quad * (b - 1), quad), quad), :] = result[quad:]
        y_copy(b).start()

    def y_wait(b):
        y_copy(b).wait_recv()

    def share_of(d, j, at, count):
        results = yy[pl.ds(pl.multiple_of(batch * (j + d - 1), batch), batch), :]
        return dot(st[d][pl.ds(at, count), :][:, :batch], results)

    def give_part(d, j, i, fresh=False):
        at = pl.multiple_of(rows * j + quad * i, quad)
        share = share_of(d, j, at, quad)
        part = rs[d].at[pl.ds(at, quad)]
        if not fresh:
            copy_to(part, part, rs_tx.at[d], rs_rv[d].at[j, i], {"ep": nxt[d]}).wait_recv()
            share = share + part[...].astype(F32)
        part[...] = share.astype(BF16)
        copy_to(part, rs[d].at[pl.ds(at - rows, quad)], rs_tx.at[d], rs_rv[d].at[j - 1, i],
                {"ep": nxt[1 - d]}).start()

    def pass_on(d, i, h):
        take_part(d, i, h)
        send_part(d, i, h + 1)

    token_load.wait()
    sort_part(0, 0)
    pl.semaphore_wait(barrier, 3)
    send_part(0, 0, 1)
    sort_part(0, 1)
    send_part(0, 1, 1)
    sort_part(0, 2)
    send_part(0, 2, 1)
    pass_on(0, 0, 1)
    sort_part(1, 0)
    send_part(1, 0, 1)
    pass_on(0, 1, 1)
    sort_part(1, 1)
    send_part(1, 1, 1)
    pass_on(0, 0, 2)
    sort_part(1, 2)
    send_part(1, 2, 1)
    sort_part(0, 3)
    send_part(0, 3, 1)
    pass_on(1, 0, 1)
    pass_on(0, 0, 3)
    pass_on(1, 1, 1)
    pass_on(0, 1, 2)
    pass_on(1, 0, 2)
    pass_on(0, 2, 1)
    sort_part(1, 3)
    blank_rows()
    for load in loads:
        load.wait()

    last = reach[0] - parts + 1

    def round_body(r, carry):
        pass_on(0, 3, r - 1)

        @pl.when(r > 2)
        def _():
            take_part(1, 3, r - 2)

        send_part(1, 3, r - 1)
        select_batch(r - 1)
        for i in range(3):
            pass_on(0, i, r + 2 - i)
            pass_on(1, i, r + 1 - i)
            if i == 1:
                expert_batch(r - 1)
        return carry

    lax.fori_loop(2, last + 1, round_body, 0)

    def y_wait_body(b, carry):
        y_wait(b)
        return carry

    order = (parts - 1,) + tuple(range(parts - 1))
    lax.fori_loop(1, last, y_wait_body, 0)
    for step in range(parts + 1):
        if step < parts:
            for d in both:
                take_part(d, order[step], reach[d] - order[step])
            select_batch(reach[0] - order[step])
        if step > 0:
            expert_batch(reach[0] - order[step - 1])
            if step > 1:
                y_wait(reach[0] - order[step - 2])
                for d in both:
                    give_part(d, reach[d] - order[step - 2], order[step - 2], True)
    y_wait(reach[0] - order[-1])
    for d in both:
        give_part(d, reach[d] - order[-1], order[-1], True)

    for i in order:
        give_part(0, reach[0] - i - 1, i)

    def give_body(r, carry):
        for i in order:
            for d in both:
                give_part(d, reach[0] - i - r, i)
        return carry

    lax.fori_loop(2, last, give_body, 0)
    for j, i in ((3, 0), (2, 1), (1, 2), (2, 0), (1, 1), (1, 0)):
        for d in both:
            give_part(d, j, i)

    def home_part(d, i):
        part = rs[d].at[pl.ds(quad * i, quad)]
        copy_to(part, part, rs_tx.at[d], rs_rv[d].at[0, i], {"ep": nxt[d]}).wait_recv()

    half = rows // 2
    own = dot(unsort[1], st1[0:rows, :]).astype(BF16)[:, :batch]
    for d in both:
        for i in range(parts // 2, parts):
            home_part(d, i)
    total[...] = (
        dot(own, yy[0:batch, :])
        + dot(unsort[0][:, half:], rs0[half:rows, :])
        + dot(unsort[1][:, half:], rs1[half:rows, :])
    )
    for i in reversed(range(parts // 2)):
        for d in both:
            home_part(d, i)
    out_ref[...] = (
        total[...] + dot(unsort[0][:, :half], rs0[0:half, :]) + dot(unsort[1][:, :half], rs1[0:half, :])
    ).astype(BF16)

    for d in both:
        moved = quad * sum(reach[d] - i for i in range(parts))
        sent = ag[d].at[pl.ds(0, moved)]
        copy_to(sent, sent, ag_tx.at[d], ag_rv[d].at[0, 0], {"ep": nxt[d]}).wait_send()
        sent = rs[d].at[pl.ds(0, moved)]
        copy_to(sent, sent, rs_tx.at[d], rs_rv[d].at[0, 0], {"ep": nxt[d]}).wait_send()
        sent = md[d].at[pl.ds(0, 8 * reach[d])]
        copy_to(sent, sent, md_tx.at[d], md_rv[d].at[0], {"ep": nxt[d]}).wait_send()
    copy_to(xout, xout, x_tx, x_rv.at[0], partner).wait_send()
    copy_to(yout, yout, y_tx, y_rv.at[0], partner).wait_send()


def local(tokens, expert_ids, route_weights, norm_gain, w_gate, w_up, w_down):
    n = lax.axis_size("ep")
    cores = lax.axis_size("tp")
    rows, width = tokens.shape
    top = expert_ids.shape[1]
    hidden_width = w_gate.shape[2]
    cap = 2 * rows * top // (n * cores)
    quad = cores * cap
    parts = rows // quad
    reach = (n // 2, n - 1 - n // 2)
    batches = reach[0]
    vmem = pl.BlockSpec(memory_space=pltpu.VMEM)
    hbm = pl.BlockSpec(memory_space=pl.ANY)
    dma = pltpu.SemaphoreType.DMA
    blocks = [pltpu.VMEM((rows * (r + 1), width), BF16) for r in reach]
    return pl.pallas_call(
        functools.partial(routed_kernel, cap),
        name="routed_layer",
        out_shape=jax.ShapeDtypeStruct((rows, width), BF16),
        in_specs=[vmem] * 3 + [hbm] * 4,
        out_specs=vmem,
        scratch_shapes=[
            pltpu.VMEM((rows, width), BF16),
            pltpu.VMEM((width, 2 * hidden_width), BF16),
            pltpu.VMEM((hidden_width, width), BF16),
            pltpu.VMEM((2, rows, rows), BF16),
            pltpu.VMEM((rows, width), F32),
            *blocks,
            *blocks,
            *[pltpu.VMEM((8 * (r + 1), rows), F32) for r in reach],
            *[pltpu.VMEM((rows * (r + 1), rows), BF16) for r in reach],
            pltpu.VMEM((2 * quad * batches, width), BF16),
            pltpu.VMEM((quad * batches, width), BF16),
            pltpu.VMEM((2 * quad * batches, width), BF16),
            pltpu.VMEM((quad * batches, width), BF16),
            dma((4,)),
            *[dma((r + 1, parts)) for r in reach],
            *[dma((r + 1, parts)) for r in reach],
            *[dma((r + 1,)) for r in reach],
            dma((batches,)),
            dma((batches,)),
            dma((2,)),
            dma((2,)),
            dma((2,)),
            dma,
            dma,
        ],
        compiler_params=pltpu.CompilerParams(
            collective_id=0, has_side_effects=True, vmem_limit_bytes=VMEM_BYTES
        ),
    )(expert_ids.T, route_weights.T, norm_gain.reshape(1, width), tokens, w_gate, w_up, w_down)


def solution(mesh):
    placed = (
        P(("grp", "ep", "tp"), None),
        P(("grp", "ep", "tp"), None),
        P(("grp", "ep", "tp"), None),
        P(),
        P(("ep", "tp"), None, None),
        P(("ep", "tp"), None, None),
        P(("ep", "tp"), None, None),
    )
    return jax.shard_map(
        local, mesh=mesh, in_specs=placed, out_specs=P(("grp", "ep", "tp"), None), check_vma=False
    )
```

time: 358 us -> 354 us (0.989)
  Pallas kernels: 356 us -> 351 us
    pallas_call x1, Pallas kernels: 356 us -> 351 us  [local(): pl.pallas_call(functools.partial(routed_kernel, cap), name='routed_layer'...]
where the time goes in v2:
time: 354 us; the launch traced here: 353 us
  Pallas kernels  351 us (99%)
    pallas_call x1, Pallas kernels, local(): pl.pallas_call(functools.partial(routed_kernel, cap), name='routed_layer'...  351 us

profile of v2, /device:TPU:37, one launch (start us, length us, event | category | flops | bytes accessed | tf_op | source)
XLA Modules:
  0.0 353.1 jit_solution(208323388168548204)
XLA Ops:
  0.0 351.2 %routed_layer.1 = bf16[128,2048]{1,0:T(8,128)(2,1)} custom-call(s32[4,128]{1,0:T(4,128)} %bitcast.4, f32[4,128]{1,0:T(4,128)} %bitcast.5, f32[1,2048]{1,0:T(1,128)} %bitcast.3, bf16[128,2048]{1,0:T(8,128)(2,1)} %tokens_hbm.1, bf16[1,2048,896]{2,1,0:T(8,128)(2,1)} %wg_hbm.1, bf16[1,2048,896]{2,1,0:T(8,128)(2,1)} %wu_hbm.1, bf16[1,896,2048]{2,1,0:T(8,128)(2,1)} %wd_hbm.1), custom_call_target="tpu_custom_call" | custom-call | tf_op jit(solution)/shard_map/routed_layer/pallas_call | solution.py:341
  351.2 1.9 copy.9
